TPU v7x, 32 devices: a whole 2x2x4 slice. The times are simulated.
32 devices in a mesh: sp: 8 (over z, y), tp: 4 (over x, core).
Axes of the slice: x: 2, y: 2, z: 4, core: 2. Of those that a mesh axis runs over, the one named last changes fastest.
Arguments:
- resid: bfloat16 [6144, 2048], P(('sp', 'tp')), may hold values from -6 to 6
- query_small: bfloat16 [6144, 768], P('sp', 'tp'), may hold values from -480 to 480
- query_large: bfloat16 [6144, 1280], P('sp', 'tp'), may hold values from -480 to 480
- kv_latent: bfloat16 [6144, 256], P('sp'), may hold values from -6 to 6
- rope_key: bfloat16 [6144, 32], P('sp'), may hold values from -6 to 6
- kv_gain: bfloat16 [256], replicated, may hold values from 0.099609375 to 1.8984375
- up_key_small: bfloat16 [256, 512], P(None, 'tp'), may hold values from -0.375 to 0.375
- up_value_small: bfloat16 [256, 512], P(None, 'tp'), may hold values from -0.375 to 0.375
- up_key_large: bfloat16 [256, 1024], P(None, 'tp'), may hold values from -0.375 to 0.375
- up_value_large: bfloat16 [256, 1024], P(None, 'tp'), may hold values from -0.375 to 0.375
- out_weight: bfloat16 [1536, 2048], replicated, may hold values from -0.359375 to 0.359375
- mix_gain: bfloat16 [2048], replicated, may hold values from 0.099609375 to 1.8984375
- gate_weight: bfloat16 [2048, 5632], P('sp', 'tp'), may hold values from -0.125 to 0.125
- up_weight: bfloat16 [2048, 5632], P('sp', 'tp'), may hold values from -0.125 to 0.125
- down_weight: bfloat16 [2048, 5632], P('sp', 'tp'), may hold values from -0.078125 to 0.078125
Outputs:
- layer_output: bfloat16 [6144, 2048], P(('sp', 'tp'))
All inputs are finite; a program needn't handle non-finite values.
Results may differ from a plain program's by a relative error of at most 0.014.
The roundings to bfloat16 on the way count: a program that leaves them out, or rounds other values in their place, can miss the bound.
Values may be sent and summed in bfloat16 or wider, within the bound.
No kernel may reach another device: no remote copies, remote signals or barrier semaphores. Data moves between devices by JAX's collectives and lax.ppermute only.
A program may use at most 128 MiB of HBM per device.

v0:
```python
import math
import jax
import jax.numpy as jnp
from jax import lax
from jax.sharding import PartitionSpec as P

HEADS_SMALL = 8
NOPE_SMALL = 64
NOPE_LARGE = 128
VALUE_SMALL = 64
VALUE_LARGE = 128
ROTARY = 32
THETA = 10000.0
EPSILON = 1e-06
FLOOR = -1e30


def angles(positions, width):
    inverse = THETA ** (-jnp.arange(0, width, 2).astype(jnp.float32) / width)
    phase = positions.astype(jnp.float32)[:, None] * inverse[None, :]
    return (jnp.cos(phase), jnp.sin(phase))


def rotate(values, angle_cos, angle_sin):
    half = values.shape[-1] // 2
    first = values[..., :half].astype(jnp.float32)
    second = values[..., half:].astype(jnp.float32)
    turned = jnp.concatenate(
        [first * angle_cos - second * angle_sin, second * angle_cos + first * angle_sin], axis=-1
    )
    return turned.astype(jnp.bfloat16)


def norm_rows(values, gain):
    wide = values.astype(jnp.float32)
    scaled = wide * lax.rsqrt(jnp.mean(wide * wide, axis=-1, keepdims=True) + EPSILON)
    return (scaled * gain.astype(jnp.float32)).astype(jnp.bfloat16)


def split_query(query, heads, nope, angle_cos, angle_sin):
    shaped = query.reshape(query.shape[0], heads, -1)
    return (
        shaped[..., :nope],
        rotate(shaped[..., nope:], angle_cos[:, None, :], angle_sin[:, None, :]),
    )


def absorb(state, query_parts, key_nope, shared_block, values, offset, first, scale):
    query_nope, query_turned = query_parts
    scores = jnp.einsum("qhd,khd->hqk", query_nope, key_nope, preferred_element_type=jnp.float32)
    scores = scores + jnp.einsum(
        "qhd,kd->hqk", query_turned, shared_block, preferred_element_type=jnp.float32
    )
    scores = scores * scale
    query_pos = offset + jnp.arange(query_nope.shape[0], dtype=jnp.int32)
    key_pos = first + jnp.arange(key_nope.shape[0], dtype=jnp.int32)
    allowed = key_pos[None, :] <= query_pos[:, None]
    scores = jnp.where(allowed[None], scores, FLOOR)
    maximum, total, summed = state
    new_max = jnp.maximum(maximum, jnp.max(scores, axis=-1))
    weights = jnp.where(allowed[None], jnp.exp(scores - new_max[..., None]), 0.0)
    factor = jnp.exp(maximum - new_max)
    total = total * factor + jnp.sum(weights, axis=-1)
    summed = summed * factor[..., None] + jnp.einsum(
        "hqk,khd->hqd", weights.astype(jnp.bfloat16), values, preferred_element_type=jnp.float32
    )
    return (new_max, total, summed)


def finish(group_state):
    maximum, total, summed = group_state
    out = summed / total[..., None]
    return jnp.transpose(out, (1, 0, 2)).reshape(out.shape[1], -1).astype(jnp.bfloat16)


def on_device(
    resid,
    query_small,
    query_large,
    kv_latent,
    rope_key,
    kv_gain,
    up_key_small,
    up_value_small,
    up_key_large,
    up_value_large,
    out_weight,
    mix_gain,
    gate_weight,
    up_weight,
    down_weight,
):
    rows = kv_latent.shape[0]
    offset = lax.axis_index("sp") * rows
    last = offset + rows - 1
    positions = offset + jnp.arange(rows, dtype=jnp.int32)
    angle_cos, angle_sin = angles(positions, ROTARY)
    latent_normed = norm_rows(kv_latent, kv_gain)
    rotated_key = rotate(rope_key, angle_cos, angle_sin)
    heads_small = up_key_small.shape[1] // NOPE_SMALL
    heads_large = up_key_large.shape[1] // NOPE_LARGE
    small_parts = split_query(query_small, heads_small, NOPE_SMALL, angle_cos, angle_sin)
    large_parts = split_query(query_large, heads_large, NOPE_LARGE, angle_cos, angle_sin)
    scale_small = 1.0 / math.sqrt(NOPE_SMALL + ROTARY)
    scale_large = 1.0 / math.sqrt(NOPE_LARGE + ROTARY)

    def start_state(heads, width):
        return (
            jnp.full((heads, rows), FLOOR, jnp.float32),
            jnp.zeros((heads, rows), jnp.float32),
            jnp.zeros((heads, rows, width), jnp.float32),
        )

    initial = (start_state(heads_small, VALUE_SMALL), start_state(heads_large, VALUE_LARGE))

    def consume(state, keys_small, values_small, keys_large, values_large, shared_block, first):
        length = shared_block.shape[0]
        small = absorb(
            state[0],
            small_parts,
            keys_small.reshape(length, heads_small, NOPE_SMALL),
            shared_block,
            values_small.reshape(length, heads_small, VALUE_SMALL),
            offset,
            first,
            scale_small,
        )
        large = absorb(
            state[1],
            large_parts,
            keys_large.reshape(length, heads_large, NOPE_LARGE),
            shared_block,
            values_large.reshape(length, heads_large, VALUE_LARGE),
            offset,
            first,
            scale_large,
        )
        return (small, large)

    def expand(latent_block):
        return tuple(
            (
                jnp.dot(latent_block, matrix, preferred_element_type=jnp.float32).astype(
                    jnp.bfloat16
                )
                for matrix in (up_key_small, up_value_small, up_key_large, up_value_large)
            )
        )

    def from_latent(blocks):
        return expand(blocks[0]) + (blocks[1],)

    pieces = (
        lax.all_gather(latent_normed, "sp", axis=0, tiled=True),
        lax.all_gather(rotated_key, "sp", axis=0, tiled=True),
    )
    count = pieces[0].shape[0] // rows

    def step(index, inner):
        first = index * rows
        blocks = tuple((lax.dynamic_slice_in_dim(piece, index * rows, rows, 0) for piece in pieces))
        return lax.cond(
            first <= last,
            lambda held: consume(held, *from_latent(blocks), first),
            lambda held: held,
            inner,
        )

    state = lax.fori_loop(0, count, step, initial)
    attn_small = finish(state[0])
    attn_large = finish(state[1])
    border = HEADS_SMALL * VALUE_SMALL
    all_small, all_large = (
        lax.all_to_all(attn_small, "tp", split_axis=0, concat_axis=1, tiled=True),
        lax.all_to_all(attn_large, "tp", split_axis=0, concat_axis=1, tiled=True),
    )
    mixed = jnp.dot(all_small, out_weight[:border], preferred_element_type=jnp.float32)
    mixed = mixed + jnp.dot(all_large, out_weight[border:], preferred_element_type=jnp.float32)
    middle = (resid.astype(jnp.float32) + mixed).astype(jnp.bfloat16)
    mixer_in = norm_rows(middle, mix_gain)
    gate_whole, up_whole, down_whole = (
        lax.all_gather(gate_weight, "sp", axis=0, tiled=True),
        lax.all_gather(up_weight, "sp", axis=0, tiled=True),
        lax.all_gather(down_weight, "sp", axis=0, tiled=True),
    )
    piece = lax.all_gather(mixer_in, "tp", axis=0, tiled=True)
    gate = jnp.dot(piece, gate_whole, preferred_element_type=jnp.float32)
    upward = jnp.dot(piece, up_whole, preferred_element_type=jnp.float32)
    hidden = (jax.nn.silu(gate) * upward).astype(jnp.bfloat16)
    branch = lax.psum_scatter(
        lax.dot_general(
            hidden, down_whole, (((1,), (1,)), ((), ())), preferred_element_type=jnp.float32
        ).astype(jnp.bfloat16),
        "tp",
        scatter_dimension=0,
        tiled=True,
    ).astype(jnp.float32)
    return (middle.astype(jnp.float32) + branch).astype(jnp.bfloat16)


def solution(mesh):
    placed = (
        P(("sp", "tp"), None),
        P("sp", "tp"),
        P("sp", "tp"),
        P("sp", None),
        P("sp", None),
        P(),
        P(None, "tp"),
        P(None, "tp"),
        P(None, "tp"),
        P(None, "tp"),
        P(),
        P(),
        P("sp", "tp"),
        P("sp", "tp"),
        P("sp", "tp"),
    )
    return jax.shard_map(
        on_device, mesh=mesh, in_specs=placed, out_specs=P(("sp", "tp"), None), check_vma=False
    )
```

profile of v0, /device:TPU:0, one launch (start us, length us, event | category | flops | bytes accessed | tf_op | source)
XLA Modules:
  0.0 495.1 jit_solution(7308712939840525357)
XLA Ops:
  8.5 1.9 fusion.46
  14.7 34.0 %all_gather.19 = bf16[6144,32]{0,1:T(8,128)(2,1)S(1)} all-gather(bf16[768,32]{0,1:T(8,128)(2,1)S(1)} %pad_maximum_fusion.2), channel_id=1, replica_groups=mesh['sp'=8,'tp'=4] {'sp'}, dimensions={0}, use_global_device_ids=true | all-gather | bytes 442368 | tf_op jit(solution)/shard_map/all_gather | solution.py:155
  48.8 26.8 %all-gather.6.cloned.1.call-done = bf16[6144,256]{1,0:T(8,128)(2,1)} async-done(((bf16[768,256]{1,0:T(8,128)(2,1)}), bf16[6144,256]{1,0:T(8,128)(2,1)}) %all-gather.6.cloned.1.call-update) | async-done | bytes 3145744 | tf_op jit(solution)/shard_map/all_gather | solution.py:154
  75.8 15.2 %while.23 = (s32[]{:T(128)}, f32[2,768]{1,0:T(2,128)S(1)}, f32[2,768]{1,0:T(2,128)S(1)}, f32[2,768,64]{1,2,0:T(8,128)S(1)}, f32[2,768]{1,0:T(2,128)S(1)}, /*inde...) while((s32[]{:T(128)}, f32[2,768]{1,0:T(2,128)S(1)}, ...), condition=%wide.region_8.9_spmd, body=%wide.region_1.8_spmd.sunk | while | flops 1384324608 | bytes 58503696 | solution.py:169
  75.8 14.9 %conditional.2 = ((f32[2,768]{1,0:T(2,128)S(1)}, f32[2,768]{1,0:T(2,128)S(1)}, f32[2,768,64]{1,2,0:T(8,128)S(1)}, f32[2,768]{1,0:T(2,128)S(1)}, f32[2,768]{1,0:T(2,128)S(1)}, /*index=5*/f32[2,768,128]{2,1,0:T(8,128)S(1)})) conditional(s32[]{:T(128)} %convert_element_type.251, (f32[2,768]{1,0:T(2,128)S(1)}, f32[2,768]{1,0:T(2,128)S(1)}, ...), branch_computations={%region_2.0_spmd, %region_3.7_spmd} | conditional | flops 1384324608 | bytes 58503288 | solution.py:162
  75.8 1.3 convolution_convert_fusion.1
  81.9 1.3 fusion.64
  83.2 1.8 fusion.7
  85.0 1.3 convolution_convert_fusion
  86.3 1.8 fusion.16
  92.7 3.5 all-to-all-start.1
  97.4 6.2 %all-to-all-done.1 = bf16[4,192,256]{2,1,0:T(8,128)(2,1)S(1)} async-done(((bf16[4,192,256]{2,1,0:T(8,128)(2,1)}), bf16[4,192,256]{2,1,0:T(8,128)(2,1)S(1)}, u32[]{:S(2)}, u32[]{:S(2)}) %all-to-all-start.1) | async-done | bytes 393248 | tf_op jit(solution)/shard_map/all_to_all | solution.py:175
  103.6 3.4 all-to-all-start
  107.2 3.2 fusion.38
  110.4 1.8 all-to-all-done
  112.2 2.5 multiply_reduce_fusion
  117.1 52.0 %all-gather.10.cloned.1.call-done = bf16[2048,1408]{1,0:T(8,128)(2,1)} async-done(((bf16[256,1408]{1,0:T(8,128)(2,1)}), bf16[2048,1408]{1,0:T(8,128)(2,1)}) %all-gather.10.cloned.1.call-update) | async-done | bytes 5767184 | tf_op jit(solution)/shard_map/all_gather | solution.py:182
  169.0 77.1 %all-gather.8.cloned.1.call-done = bf16[768,2048]{1,0:T(8,128)(2,1)} async-done(((bf16[192,2048]{1,0:T(8,128)(2,1)}), bf16[768,2048]{1,0:T(8,128)(2,1)}) %all-gather.8.cloned.1.call-update) | async-done | bytes 3145744 | tf_op jit(solution)/shard_map/all_gather | solution.py:186
  246.1 9.7 %fusion.68 = f32[768,1408]{1,0:T(8,128)} fusion(bf16[768,2048]{1,0:T(8,128)(2,1)} %all-gather.8.cloned.1.call-done, bf16[2048,1408]{1,0:T(8,128)(2,1)} %all-gather.10.cloned.1.call-done), kind=kOutput, calls=%fused_computation.108 | convolution fusion | flops 4429185024 | bytes 13238272 | tf_op jit(solution)/shard_map/dot_general | solution.py:187
  255.8 84.7 %all-gather.12.cloned.1.call-done = bf16[2048,1408]{1,0:T(8,128)(2,1)} async-done(((bf16[256,1408]{1,0:T(8,128)(2,1)}), bf16[2048,1408]{1,0:T(8,128)(2,1)}) %all-gather.12.cloned.1.call-update) | async-done | bytes 5767184 | tf_op jit(solution)/shard_map/all_gather | solution.py:183
  340.5 92.6 %all-gather.14.cloned.1.call-done = bf16[2048,1408]{1,0:T(8,128)(2,1)} async-done(((bf16[256,1408]{1,0:T(8,128)(2,1)}), bf16[2048,1408]{1,0:T(8,128)(2,1)}) %all-gather.14.cloned.1.call-update) | async-done | bytes 5767184 | tf_op jit(solution)/shard_map/all_gather | solution.py:184
  433.1 16.7 %convolution_convert_fusion.4 = bf16[768,2048]{1,0:T(8,128)(2,1)} fusion(bf16[2048,1408]{1,0:T(8,128)(2,1)} %all-gather.14.cloned.1.call-done, f32[768,1408]{1,0:T(8,128)} %fusion.68, bf16[768,2048]{1,0:T(8,128)(2,1)} %all-gather.8.cloned.1.call-done, bf16[2048,1408]{1,0:T(8,128)(2,1)} %all-gather.12.cloned.1.call-done), kind=kOutput, calls=%fused_computation.50 | convolution fusion | flops 8866430976 | bytes 22151168 | tf_op jit(solution)/shard_map/dot_general | solution.py:191
  449.8 36.2 %reduce-scatter.2.cloned.1.call-done = bf16[192,2048]{1,0:T(8,128)(2,1)} async-done(((bf16[768,2048]{1,0:T(8,128)(2,1)}), bf16[192,2048]{1,0:T(8,128)(2,1)}) %reduce-scatter.2.cloned.1.call-update) | async-done | bytes 786448 | tf_op jit(solution)/shard_map/reduce_scatter | solution.py:190
  486.0 2.2 add_convert_fusion
  (73 shorter events, 19.1 us)
Async XLA Ops:
  6.5 6.9 %copy-start.4 = (bf16[768,32]{0,1:T(8,128)(2,1)S(1)}, bf16[768,32]{0,1:T(8,128)(2,1)}, u32[]{:S(2)}) copy-start(bf16[768,32]{0,1:T(8,128)(2,1)} %param.23) | copy-start | bytes 147460
  6.5 69.2 %copy-start.2 = (bf16[256,128]{1,0:T(8,128)(2,1)S(1)}, bf16[256,128]{1,0:T(8,128)(2,1)}, u32[]{:S(2)}) copy-start(bf16[256,128]{1,0:T(8,128)(2,1)} %param.25) | copy-start | bytes 196612
  6.5 69.2 %copy-start.3 = (bf16[256,128]{1,0:T(8,128)(2,1)S(1)}, bf16[256,128]{1,0:T(8,128)(2,1)}, u32[]{:S(2)}) copy-start(bf16[256,128]{1,0:T(8,128)(2,1)} %param.26) | copy-start | bytes 196612
  6.5 69.2 %copy-start = (bf16[256,256]{1,0:T(8,128)(2,1)S(1)}, bf16[256,256]{1,0:T(8,128)(2,1)}, u32[]{:S(2)}) copy-start(bf16[256,256]{1,0:T(8,128)(2,1)} %param.27) | copy-start | bytes 393220
  6.5 69.2 %copy-start.1 = (bf16[256,256]{1,0:T(8,128)(2,1)S(1)}, bf16[256,256]{1,0:T(8,128)(2,1)}, u32[]{:S(2)}) copy-start(bf16[256,256]{1,0:T(8,128)(2,1)} %param.28) | copy-start | bytes 393220
  6.5 69.0 %all-gather.6.cloned.1.call-start = ((), (), s32[]{:S(2)}) async-start(), calls=%async_computation.3 | async-start | bytes 3538944 | tf_op jit(solution)/shard_map/all_gather | solution.py:154
  10.5 158.6 %all-gather.10.cloned.1.call-start = ((), (), s32[]{:S(2)}) async-start(), calls=%async_computation.5 | async-start | bytes 6488064 | tf_op jit(solution)/shard_map/all_gather | solution.py:182
  75.8 20.4 %copy-start.5 = (bf16[2048]{0:T(1024)(128)(2,1)S(1)}, bf16[2048]{0:T(1024)(128)(2,1)}, u32[]{:S(2)}) copy-start(bf16[2048]{0:T(1024)(128)(2,1)} %param.30) | copy-start | bytes 12292
  92.7 10.8 %all-to-all-start.1 = ((bf16[4,192,256]{2,1,0:T(8,128)(2,1)}), bf16[4,192,256]{2,1,0:T(8,128)(2,1)S(1)}, u32[]{:S(2)}, u32[]{:S(2)}) async-start(bf16[4,192,256]{2,1,0:T(8,128)(2,1)} %convert_element_type.152), calls=%async_computation.1 | async-start | bytes 786432 | tf_op jit(solution)/shard_map/all_to_all | solution.py:175
  103.6 8.6 %all-to-all-start = ((bf16[4,192,128]{2,1,0:T(8,128)(2,1)}), bf16[4,192,128]{2,1,0:T(8,128)(2,1)S(1)}, u32[]{:S(2)}, u32[]{:S(2)}) async-start(bf16[4,192,128]{2,1,0:T(8,128)(2,1)} %copy.34), calls=%async_computation | async-start | bytes 393216 | tf_op jit(solution)/shard_map/all_to_all | solution.py:174
  107.0 139.2 %all-gather.8.cloned.1.call-start = ((), (), s32[]{:S(2)}) async-start(), calls=%async_computation.4 | async-start | bytes 3932160 | tf_op jit(solution)/shard_map/all_gather | solution.py:186
  115.9 224.7 %all-gather.12.cloned.1.call-start = ((), (), s32[]{:S(2)}) async-start(), calls=%async_computation.6 | async-start | bytes 6488064 | tf_op jit(solution)/shard_map/all_gather | solution.py:183
  116.4 316.6 %all-gather.14.cloned.1.call-start = ((), (), s32[]{:S(2)}) async-start(), calls=%async_computation.7 | async-start | bytes 6488064 | tf_op jit(solution)/shard_map/all_gather | solution.py:184
  117.0 369.0 %reduce-scatter.2.cloned.1.call-start = ((), (), s32[]{:S(2)}) async-start(), calls=%async_computation.8 | async-start | bytes 3932160 | tf_op jit(solution)/shard_map/reduce_scatter | solution.py:190
Sparse Core Ops, SparseCore 0:
  10.6 64.9 all-gather.5
  77.8 91.2 all-gather.9
  170.6 75.4 all-gather.7
  248.2 92.3 all-gather.11
  342.6 90.4 all-gather.13
  449.9 36.0 reduce-scatter.1
where the time goes:
time: 497 us; the launch traced here: 495 us
  waiting for transfers between devices  379 us (76%)
  matrix products  44.7 us (9%)
  blocking collectives  34 us (7%)
  between operations  13.7 us (3%)
  other arithmetic  10.9 us (2%)
  starting transfers between devices  7.25 us (1%)
    all_gather x1, waiting for transfers between devices, on_device(): lax.all_gather(down_weight, 'sp', axis=0, tiled=True)  92.6 us
    all_gather x1, waiting for transfers between devices, on_device(): lax.all_gather(up_weight, 'sp', axis=0, tiled=True)  84.7 us
    all_gather x1, waiting for transfers between devices, on_device(): piece = lax.all_gather(mixer_in, 'tp', axis=0, tiled=True)  77.1 us
    all_gather x1, waiting for transfers between devices, on_device(): lax.all_gather(gate_weight, 'sp', axis=0, tiled=True)  52 us
    reduce_scatter x1, waiting for transfers between devices, on_device(): lax.psum_scatter(lax.dot_general(hidden, down_whole, (((1,), (1,)), ((),...  36.2 us
    all_gather x1, blocking collectives, on_device(): lax.all_gather(rotated_key, 'sp', axis=0, tiled=True)  34 us
    all_gather x1, waiting for transfers between devices, on_device(): lax.all_gather(latent_normed, 'sp', axis=0, tiled=True)  26.8 us
    dot_general x1, matrix products, on_device(): lax.dot_general(hidden, down_whole, (((1,), (1,)), ((), ())), preferred_e...  16.7 us
  transfers between devices with their start and end apart: 8, of which 8 were waited for; matrix products, arithmetic and copies ran while one was open for 8% of the time, Pallas kernels for 0%

commit v1 on v0

--- a/solution.py
+++ b/solution.py
@@ -183,7 +183,13 @@
         lax.all_gather(up_weight, "sp", axis=0, tiled=True),
         lax.all_gather(down_weight, "sp", axis=0, tiled=True),
     )
-    piece = lax.all_gather(mixer_in, "tp", axis=0, tiled=True)
+    count_2 = lax.axis_size("tp")
+    moving, tiles = (mixer_in, [mixer_in])
+    for _ in range(count_2 - 1):
+        moving = lax.ppermute(moving, "tp", [(i, (i + 1) % count_2) for i in range(count_2)])
+        tiles.insert(0, moving)
+    line = jnp.concatenate(tiles, axis=0)
+    piece = jnp.roll(line, (lax.axis_index("tp") + 1) * mixer_in.shape[0], axis=0)
     gate = jnp.dot(piece, gate_whole, preferred_element_type=jnp.float32)
     upward = jnp.dot(piece, up_whole, preferred_element_type=jnp.float32)
     hidden = (jax.nn.silu(gate) * upward).astype(jnp.bfloat16)

time: 497 us -> 418 us (0.84)
  waiting for transfers between devices: 379 us -> 292 us
  local copies, waits for them, and re-layouts: 4.89 us -> 12 us
    all_gather x1 -> x0, waiting for transfers between devices: 77.1 us -> none  [on_device(): piece = lax.all_gather(mixer_in, 'tp', axis=0, tiled=True)]
    all_gather x1, waiting for transfers between devices: 52 us -> 9.36 us  [on_device(): lax.all_gather(gate_weight, 'sp', axis=0, tiled=True)]
    ppermute x0 -> x3, waiting for transfers between devices: none -> 34.3 us  [on_device(): lax.ppermute(moving, 'tp', [(i, (i + 1) % count_2) for i in range(count_2)])]
    all_gather x1, waiting for transfers between devices: 92.6 us -> 83 us  [on_device(): lax.all_gather(down_weight, 'sp', axis=0, tiled=True)]
    unnamed x12 -> x20, local copies, waits for them, and re-layouts: 0.02 us -> 8.11 us
    all_gather x1, waiting for transfers between devices: 84.7 us -> 92.6 us  [on_device(): lax.all_gather(up_weight, 'sp', axis=0, tiled=True)]
  transfers between devices with their start and end apart: 8 -> 10, of which waited for: 8 -> 10; matrix products, arithmetic and copies ran while one was open for 8% -> 11% of each run, Pallas kernels for 0% -> 0%
where the time goes in v1:
time: 418 us; the launch traced here: 416 us
  waiting for transfers between devices  292 us (70%)
  matrix products  44.7 us (11%)
  blocking collectives  34.1 us (8%)
  between operations  13.4 us (3%)
  other arithmetic  12.2 us (3%)
  local copies, waits for them, and re-layouts  12 us (3%)
  starting transfers between devices  7.27 us (2%)
    all_gather x1, waiting for transfers between devices, on_device(): lax.all_gather(up_weight, 'sp', axis=0, tiled=True)  92.6 us
    all_gather x1, waiting for transfers between devices, on_device(): lax.all_gather(down_weight, 'sp', axis=0, tiled=True)  83 us
    reduce_scatter x1, waiting for transfers between devices, on_device(): lax.psum_scatter(lax.dot_general(hidden, down_whole, (((1,), (1,)), ((),...  36.2 us
    ppermute x3, waiting for transfers between devices, on_device(): lax.ppermute(moving, 'tp', [(i, (i + 1) % count_2) for i in range(count_2)])  34.3 us
    all_gather x1, blocking collectives, on_device(): lax.all_gather(rotated_key, 'sp', axis=0, tiled=True)  34.1 us
    all_gather x1, waiting for transfers between devices, on_device(): lax.all_gather(latent_normed, 'sp', axis=0, tiled=True)  26.4 us
    dot_general x1, matrix products, on_device(): lax.dot_general(hidden, down_whole, (((1,), (1,)), ((), ())), preferred_e...  16.8 us
    dot_general x1, matrix products, on_device(): gate = jnp.dot(piece, gate_whole, preferred_element_type=jnp.float32)  9.69 us
  transfers between devices with their start and end apart: 10, of which 10 were waited for; matrix products, arithmetic and copies ran while one was open for 11% of the time, Pallas kernels for 0%

profile of v1, /device:TPU:0, one launch (start us, length us, event | category | flops | bytes accessed | tf_op | source)
XLA Modules:
  0.0 416.3 jit_solution(11130720606319636396)
XLA Ops:
  8.5 1.9 fusion.54
  15.0 34.1 %all_gather.16 = bf16[6144,32]{0,1:T(8,128)(2,1)S(1)} all-gather(bf16[768,32]{0,1:T(8,128)(2,1)S(1)} %pad_maximum_fusion.2), channel_id=1, replica_groups=mesh['sp'=8,'tp'=4] {'sp'}, dimensions={0}, use_global_device_ids=true | all-gather | bytes 442368 | tf_op jit(solution)/shard_map/all_gather | solution.py:155
  49.2 26.4 %all-gather.5.cloned.1.call-done = bf16[6144,256]{1,0:T(8,128)(2,1)} async-done(((bf16[768,256]{1,0:T(8,128)(2,1)}), bf16[6144,256]{1,0:T(8,128)(2,1)}) %all-gather.5.cloned.1.call-update) | async-done | bytes 3145744 | tf_op jit(solution)/shard_map/all_gather | solution.py:154
  75.8 15.3 %while.23 = (s32[]{:T(128)}, f32[2,768]{1,0:T(2,128)S(1)}, f32[2,768]{1,0:T(2,128)S(1)}, f32[2,768,64]{1,2,0:T(8,128)S(1)}, f32[2,768]{1,0:T(2,128)S(1)}, /*inde...) while((s32[]{:T(128)}, f32[2,768]{1,0:T(2,128)S(1)}, ...), condition=%wide.region_8.9_spmd, body=%wide.region_1.8_spmd.sunk | while | flops 1384324608 | bytes 58503696 | solution.py:169
  75.8 14.9 %conditional.2 = ((f32[2,768]{1,0:T(2,128)S(1)}, f32[2,768]{1,0:T(2,128)S(1)}, f32[2,768,64]{1,2,0:T(8,128)S(1)}, f32[2,768]{1,0:T(2,128)S(1)}, f32[2,768]{1,0:T(2,128)S(1)}, /*index=5*/f32[2,768,128]{2,1,0:T(8,128)S(1)})) conditional(s32[]{:T(128)} %convert_element_type.255, (f32[2,768]{1,0:T(2,128)S(1)}, f32[2,768]{1,0:T(2,128)S(1)}, ...), branch_computations={%region_2.0_spmd, %region_3.7_spmd} | conditional | flops 1384324608 | bytes 58503288 | solution.py:162
  83.1 1.8 fusion.7
  92.8 3.5 all-to-all-start.1
  97.4 6.2 %all-to-all-done.1 = bf16[4,192,256]{2,1,0:T(8,128)(2,1)S(1)} async-done(((bf16[4,192,256]{2,1,0:T(8,128)(2,1)}), bf16[4,192,256]{2,1,0:T(8,128)(2,1)S(1)}, u32[]{:S(2)}, u32[]{:S(2)}) %all-to-all-start.1) | async-done | bytes 393248 | tf_op jit(solution)/shard_map/all_to_all | solution.py:175
  103.6 3.5 all-to-all-start
  107.3 3.2 fusion.38
  110.4 2.0 all-to-all-done
  112.4 2.6 multiply_reduce_fusion
  115.3 11.4 %collective-permute-done = bf16[192,2048]{1,0:T(8,128)(2,1)S(1)} collective-permute-done((bf16[192,2048]{1,0:T(8,128)(2,1)S(1)}, bf16[192,2048]{1,0:T(8,128)(2,1)S(1)}, u32[]{:S(2)}, u32[]{:S(2)}) %collective-permute-start) | collective-permute-done | bytes 786464 | tf_op jit(solution)/shard_map/ppermute | solution.py:189
  126.7 11.4 %collective-permute-done.1 = bf16[192,2048]{1,0:T(8,128)(2,1)S(1)} collective-permute-done((bf16[192,2048]{1,0:T(8,128)(2,1)S(1)}, bf16[192,2048]{1,0:T(8,128)(2,1)S(1)}, u32[]{:S(2)}, u32[]{:S(2)}) %collective-permute-start.1) | collective-permute-done | bytes 786464 | tf_op jit(solution)/shard_map/ppermute | solution.py:189
  138.1 11.5 %collective-permute-done.2 = bf16[192,2048]{1,0:T(8,128)(2,1)} collective-permute-done((bf16[192,2048]{1,0:T(8,128)(2,1)S(1)}, bf16[192,2048]{1,0:T(8,128)(2,1)}, u32[]{:S(2)}, u32[]{:S(2)}) %collective-permute-start.2) | collective-permute-done | bytes 786464 | tf_op jit(solution)/shard_map/ppermute | solution.py:189
  149.7 2.1 constant_dynamic-update-slice_fusion.7
  154.8 2.1 constant_dynamic-update-slice_fusion.3
  159.9 9.4 %all-gather.7.cloned.1.call-done = bf16[2048,1408]{1,0:T(8,128)(2,1)} async-done(((bf16[256,1408]{1,0:T(8,128)(2,1)}), bf16[2048,1408]{1,0:T(8,128)(2,1)}) %all-gather.7.cloned.1.call-update) | async-done | bytes 5767184 | tf_op jit(solution)/shard_map/all_gather | solution.py:182
  169.3 9.7 %fusion.42 = f32[768,1408]{1,0:T(8,128)} fusion(bf16[2048,1408]{1,0:T(8,128)(2,1)} %all-gather.7.cloned.1.call-done, bf16[1536,2048]{1,0:T(8,128)(2,1)} %constant_dynamic-update-slice_fusion, s32[]{:T(128)S(6)} %select_n.49), kind=kOutput, calls=%fused_computation.53 | convolution fusion | flops 4429185024 | bytes 13238276 | tf_op jit(solution)/shard_map/dot_general | solution.py:193
  179.0 83.0 %all-gather.11.cloned.1.call-done = bf16[2048,1408]{1,0:T(8,128)(2,1)} async-done(((bf16[256,1408]{1,0:T(8,128)(2,1)}), bf16[2048,1408]{1,0:T(8,128)(2,1)}) %all-gather.11.cloned.1.call-update) | async-done | bytes 5767184 | tf_op jit(solution)/shard_map/all_gather | solution.py:184
  262.0 92.6 %all-gather.9.cloned.1.call-done = bf16[2048,1408]{1,0:T(8,128)(2,1)} async-done(((bf16[256,1408]{1,0:T(8,128)(2,1)}), bf16[2048,1408]{1,0:T(8,128)(2,1)}) %all-gather.9.cloned.1.call-update) | async-done | bytes 5767184 | tf_op jit(solution)/shard_map/all_gather | solution.py:183
  354.6 16.8 %convolution_convert_fusion.4 = bf16[768,2048]{1,0:T(8,128)(2,1)} fusion(bf16[2048,1408]{1,0:T(8,128)(2,1)} %all-gather.11.cloned.1.call-done, f32[768,1408]{1,0:T(8,128)} %fusion.42, bf16[2048,1408]{1,0:T(8,128)(2,1)} %all-gather.9.cloned.1.call-done, bf16[1536,2048]{1,0:T(8,128)(2,1)} %constant_dynamic-update-slice_fusion, s32[]{:T(128)S(6)} %select_n.49), kind=kOutput, calls=%fused_computation.50 | convolution fusion | flops 8866430976 | bytes 22151172 | tf_op jit(solution)/shard_map/dot_general | solution.py:197
  371.4 36.2 %reduce-scatter.2.cloned.1.call-done = bf16[192,2048]{1,0:T(8,128)(2,1)} async-done(((bf16[768,2048]{1,0:T(8,128)(2,1)}), bf16[192,2048]{1,0:T(8,128)(2,1)}) %reduce-scatter.2.cloned.1.call-update) | async-done | bytes 786448 | tf_op jit(solution)/shard_map/reduce_scatter | solution.py:196
  407.6 2.2 add_convert_fusion
  (86 shorter events, 28.9 us)
Async XLA Ops:
  6.5 7.2 %copy-start.4 = (bf16[768,192]{0,1:T(8,128)(2,1)S(1)}, bf16[768,192]{0,1:T(8,128)(2,1)}, u32[]{:S(2)}) copy-start(bf16[768,192]{0,1:T(8,128)(2,1)} %param.20) | copy-start | bytes 884740
  6.5 7.3 %copy-start.5 = (bf16[768,32]{0,1:T(8,128)(2,1)S(1)}, bf16[768,32]{0,1:T(8,128)(2,1)}, u32[]{:S(2)}) copy-start(bf16[768,32]{0,1:T(8,128)(2,1)} %param.23) | copy-start | bytes 147460
  6.5 69.2 %copy-start.2 = (bf16[256,128]{1,0:T(8,128)(2,1)S(1)}, bf16[256,128]{1,0:T(8,128)(2,1)}, u32[]{:S(2)}) copy-start(bf16[256,128]{1,0:T(8,128)(2,1)} %param.25) | copy-start | bytes 196612
  6.5 69.2 %copy-start.3 = (bf16[256,128]{1,0:T(8,128)(2,1)S(1)}, bf16[256,128]{1,0:T(8,128)(2,1)}, u32[]{:S(2)}) copy-start(bf16[256,128]{1,0:T(8,128)(2,1)} %param.26) | copy-start | bytes 196612
  6.5 69.2 %copy-start = (bf16[256,256]{1,0:T(8,128)(2,1)S(1)}, bf16[256,256]{1,0:T(8,128)(2,1)}, u32[]{:S(2)}) copy-start(bf16[256,256]{1,0:T(8,128)(2,1)} %param.27) | copy-start | bytes 393220
  6.5 69.2 %copy-start.1 = (bf16[256,256]{1,0:T(8,128)(2,1)S(1)}, bf16[256,256]{1,0:T(8,128)(2,1)}, u32[]{:S(2)}) copy-start(bf16[256,256]{1,0:T(8,128)(2,1)} %param.28) | copy-start | bytes 393220
  6.6 69.0 %all-gather.5.cloned.1.call-start = ((), (), s32[]{:S(2)}) async-start(), calls=%async_computation.3 | async-start | bytes 3538944 | tf_op jit(solution)/shard_map/all_gather | solution.py:154
  10.4 158.8 %all-gather.7.cloned.1.call-start = ((), (), s32[]{:S(2)}) async-start(), calls=%async_computation.4 | async-start | bytes 6488064 | tf_op jit(solution)/shard_map/all_gather | solution.py:182
  11.2 250.8 %all-gather.11.cloned.1.call-start = ((), (), s32[]{:S(2)}) async-start(), calls=%async_computation.6 | async-start | bytes 6488064 | tf_op jit(solution)/shard_map/all_gather | solution.py:184
  11.9 342.6 %all-gather.9.cloned.1.call-start = ((), (), s32[]{:S(2)}) async-start(), calls=%async_computation.5 | async-start | bytes 6488064 | tf_op jit(solution)/shard_map/all_gather | solution.py:183
  75.8 20.5 %copy-start.6 = (bf16[2048]{0:T(1024)(128)(2,1)S(1)}, bf16[2048]{0:T(1024)(128)(2,1)}, u32[]{:S(2)}) copy-start(bf16[2048]{0:T(1024)(128)(2,1)} %param.30) | copy-start | bytes 12292
  92.8 10.8 %all-to-all-start.1 = ((bf16[4,192,256]{2,1,0:T(8,128)(2,1)}), bf16[4,192,256]{2,1,0:T(8,128)(2,1)S(1)}, u32[]{:S(2)}, u32[]{:S(2)}) async-start(bf16[4,192,256]{2,1,0:T(8,128)(2,1)} %convert_element_type.152), calls=%async_computation.1 | async-start | bytes 786432 | tf_op jit(solution)/shard_map/all_to_all | solution.py:175
  103.6 8.8 %all-to-all-start = ((bf16[4,192,128]{2,1,0:T(8,128)(2,1)}), bf16[4,192,128]{2,1,0:T(8,128)(2,1)S(1)}, u32[]{:S(2)}, u32[]{:S(2)}) async-start(bf16[4,192,128]{2,1,0:T(8,128)(2,1)} %copy.34), calls=%async_computation | async-start | bytes 393216 | tf_op jit(solution)/shard_map/all_to_all | solution.py:174
  107.2 300.4 %reduce-scatter.2.cloned.1.call-start = ((), (), s32[]{:S(2)}) async-start(), calls=%async_computation.7 | async-start | bytes 3932160 | tf_op jit(solution)/shard_map/reduce_scatter | solution.py:196
  115.3 11.5 %collective-permute-start = (bf16[192,2048]{1,0:T(8,128)(2,1)S(1)}, bf16[192,2048]{1,0:T(8,128)(2,1)S(1)}, u32[]{:S(2)}, u32[]{:S(2)}) collective-permute-start(bf16[192,2048]{1,0:T(8,128)(2,1)S(1)} %multiply_convert_fusion.1), channel_id=1, source_target_pairs={{0,1},{1,2},{2,3},{3,0},{4,5},{5,6},{6,7},{7,4},{8,9},{9,10},{10,1... | collective-permute-start | bytes 2359304 | tf_op jit(solution)/shard_map/ppermute | solution.py:189
  126.7 11.4 %collective-permute-start.1 = (bf16[192,2048]{1,0:T(8,128)(2,1)S(1)}, bf16[192,2048]{1,0:T(8,128)(2,1)S(1)}, u32[]{:S(2)}, u32[]{:S(2)}) collective-permute-start(bf16[192,2048]{1,0:T(8,128)(2,1)S(1)} %collective-permute-done), channel_id=1, source_target_pairs={{0,1},{1,2},{2,3},{3,0},{4,5},{5,6},{6,7},{7,4},{8,9},{9,10},{10,1... | collective-permute-start | bytes 2359304 | tf_op jit(solution)/shard_map/ppermute | solution.py:189
  138.1 11.5 %collective-permute-start.2 = (bf16[192,2048]{1,0:T(8,128)(2,1)S(1)}, bf16[192,2048]{1,0:T(8,128)(2,1)}, u32[]{:S(2)}, u32[]{:S(2)}) collective-permute-start(bf16[192,2048]{1,0:T(8,128)(2,1)S(1)} %collective-permute-done.1), channel_id=1, source_target_pairs={{0,1},{1,2},{2,3},{3,0},{4,5},{5,6},{6,7},{7,4},{8,9},{9,10},{10,1... | collective-permute-start | bytes 2359304 | tf_op jit(solution)/shard_map/ppermute | solution.py:189
Sparse Core Ops, SparseCore 0:
  10.6 64.9 all-gather.4
  77.8 91.4 all-gather.6
  171.5 90.4 all-gather.10
  264.0 90.4 all-gather.8
  371.5 36.0 reduce-scatter.1
